TPU v7x, 32 devices: a whole 2x2x4 slice. The times are simulated.
32 devices in a mesh: ra: 8 (over z, y), cb: 4 (over x, core).
Axes of the slice: x: 2, y: 2, z: 4, core: 2. Of those that a mesh axis runs over, the one named last changes fastest.
Arguments:
- tokens: bfloat16 [512, 4096], P(None, 'cb'), may hold values from -400 to 400
- norm_gain: bfloat16 [4096], P('cb'), may hold values from 0.099609375 to 1.8984375
- w_gate: bfloat16 [4096, 11264], P('cb', 'ra'), may hold values from -0.09375 to 0.09375
- w_up: bfloat16 [4096, 11264], P('cb', 'ra'), may hold values from -0.09375 to 0.09375
- w_down: bfloat16 [11264, 4096], P('ra', 'cb'), may hold values from -0.0546875 to 0.0546875
- out_gain: bfloat16 [4096], P('cb'), may hold values from 0.099609375 to 1.8984375
Outputs:
- normed_out: bfloat16 [512, 4096], P('ra', 'cb')
All inputs are finite; a program needn't handle non-finite values.
Results may differ from a plain program's by a relative error of at most 0.0045.
Values sent between devices are 32-bit elements; how exact they have to be, the bound alone decides.
A program may use at most 64 MiB of HBM per device.

v0:
```python
import jax
import jax.numpy as jnp
from jax import lax
from jax.sharding import PartitionSpec as P

D = 4096


def body(tokens, norm_gain, w_gate, w_up, w_down, out_gain):
    eps = 1e-06
    xfloat = tokens.astype(jnp.float32)
    local_sq = jnp.sum(xfloat * xfloat, axis=1)
    scaled = (xfloat * norm_gain.astype(jnp.float32)).astype(jnp.bfloat16)
    gate_part = jnp.dot(scaled, w_gate, preferred_element_type=jnp.float32)
    up_part = jnp.dot(scaled, w_up, preferred_element_type=jnp.float32)
    total_sq, gate_sum, up_sum = lax.psum((local_sq, gate_part, up_part), "cb")
    inv_in = lax.rsqrt(total_sq / D + eps)[:, None]
    hidden = (jax.nn.silu(gate_sum * inv_in) * (up_sum * inv_in)).astype(jnp.bfloat16)
    partial_down = jnp.dot(hidden, w_down, preferred_element_type=jnp.float32)
    own_rows = tokens.shape[0] // lax.axis_size("ra")
    first_row = lax.axis_index("ra") * own_rows
    down = lax.psum_scatter(partial_down, "ra", scatter_dimension=0, tiled=True)
    residual = lax.dynamic_slice_in_dim(xfloat, first_row, own_rows, 0)
    mixed = 0.1 * residual + down
    out_sq = lax.psum(jnp.sum(mixed * mixed, axis=1), "cb")
    inv_out = lax.rsqrt(out_sq / D + eps)[:, None]
    return (mixed * inv_out * out_gain.astype(jnp.float32)).astype(jnp.bfloat16)


def solution(mesh):
    return jax.shard_map(
        body,
        mesh=mesh,
        in_specs=(P(None, "cb"), P("cb"), P("cb", "ra"), P("cb", "ra"), P("ra", "cb"), P("cb")),
        out_specs=P("ra", "cb"),
        check_vma=False,
    )
```

profile of v0, /device:TPU:0, one launch (start us, length us, event | category | flops | bytes accessed | tf_op | source)
XLA Modules:
  0.0 221.7 jit_solution(3549083786909565861)
XLA Ops:
  6.5 0.0 copy-start
  6.5 0.0 all-reduce.3.cloned.1.call-start
  6.5 0.8 convert_element_type.19
  7.4 1.0 copy-done
  8.4 0.0 copy-start.1
  8.4 0.0 copy-start.3
  8.4 4.7 %fusion.1 = f32[512,1408]{1,0:T(8,128)} fusion(bf16[1024,1408]{1,0:T(8,128)(2,1)S(1)} %copy-done, f32[1024]{0:T(1024)S(1)} %convert_element_type.19, bf16[512,1024]{1,0:T(8,128)(2,1)} %param.6), kind=kOutput, calls=%fused_computation.4 | convolution fusion | flops 1477967872 | bytes 6819840 | tf_op jit(solution)/shard_map/dot_general | solution.py:15
  13.1 0.0 copy-done.1
  13.1 0.0 copy-done.3
  13.1 3.5 %fusion.2 = f32[512,1408]{1,0:T(8,128)} fusion(bf16[1024,1408]{1,0:T(8,128)(2,1)S(1)} %copy-done.3, f32[1024]{0:T(1024)S(1)} %convert_element_type.19, bf16[512,1024]{1,0:T(8,128)(2,1)S(1)} %copy-done.1), kind=kOutput, calls=%fused_computation.5 | convolution fusion | flops 1477967872 | bytes 6819840 | tf_op jit(solution)/shard_map/dot_general | solution.py:14
  16.6 0.0 all-reduce.3.cloned.1.call-update
  16.6 0.0 reduce-scatter.2.cloned.1.call-start
  16.6 1.5 multiply_reduce_fusion
  18.1 8.4 %psum.29 = f32[512]{0:T(512)S(1)} all-reduce(f32[512]{0:T(512)S(1)} %multiply_reduce_fusion), channel_id=1, replica_groups=mesh['ra'=8,'cb'=4] {'cb'}, use_global_device_ids=true, to_apply=%region_2.0 | all-reduce | flops 512 | bytes 4096 | tf_op jit(solution)/shard_map/psum | solution.py:16
  26.5 104.0 %all-reduce.3.cloned.1.call-done = (f32[512,1408]{1,0:T(8,128)}, f32[512,1408]{1,0:T(8,128)}) async-done(((f32[512,1408]{1,0:T(8,128)}, f32[512,1408]{1,0:T(8,128)}), (f32[512,1408]{1,0:T(8,128)}, f32[512,1408]{1,0:T(8,128)})) %all-reduce.3.cloned.1.call-update) | async-done | bytes 5767184 | tf_op jit(solution)/shard_map/psum | solution.py:16
  130.5 6.8 %fusion = f32[512,1024]{1,0:T(8,128)} fusion(bf16[1408,1024]{1,0:T(8,128)(2,1)} %param.10, f32[512,1408]{1,0:T(8,128)} %get-tuple-element.5, f32[512,1408]{1,0:T(8,128)} %get-tuple-element.6, f32[512]{0:T(512)S(1)} %add_rsqrt_fusion), kind=kOutput, calls=%fused_computation.3 | convolution fusion | flops 1482162176 | bytes 10749952 | tf_op jit(solution)/shard_map/dot_general | solution.py:19
  137.4 0.0 copy-start.2
  137.4 0.0 reduce-scatter.2.cloned.1.call-update
  137.4 2.8 %convert_element_type.18 = f32[512,1024]{1,0:T(8,128)} convert(bf16[512,1024]{1,0:T(8,128)(2,1)} %param.6) | non-fusion elementwise | flops 524288 | bytes 3145728 | tf_op jit(solution)/shard_map/convert_element_type | solution.py:11
  140.2 0.0 copy-done.2
  140.2 66.0 %reduce-scatter.2.cloned.1.call-done = f32[64,1024]{1,0:T(8,128)} async-done(((f32[512,1024]{1,0:T(8,128)}), f32[64,1024]{1,0:T(8,128)}) %reduce-scatter.2.cloned.1.call-update) | async-done | bytes 262160 | tf_op jit(solution)/shard_map/reduce_scatter | solution.py:22
  206.2 1.2 multiply_reduce_fusion.1
  207.4 5.7 %psum.31 = f32[64]{0:T(128)S(1)} all-reduce(f32[64]{0:T(128)S(1)} %multiply_reduce_fusion.1), channel_id=1, replica_groups=mesh['ra'=8,'cb'=4] {'cb'}, use_global_device_ids=true, to_apply=%region_6.7 | all-reduce | flops 64 | bytes 512 | tf_op jit(solution)/shard_map/psum | solution.py:25
  213.0 1.8 multiply_convert_fusion.5
  (3 shorter events, 0.0 us)
Async XLA Ops:
  6.5 1.8 copy-start
  6.5 124.0 %all-reduce.3.cloned.1.call-start = ((), (), s32[]{:S(2)}) async-start(), calls=%async_computation.2 | async-start | bytes 11534336 | tf_op jit(solution)/shard_map/psum | solution.py:16
  8.4 4.7 %copy-start.1 = (bf16[512,1024]{1,0:T(8,128)(2,1)S(1)}, bf16[512,1024]{1,0:T(8,128)(2,1)}, u32[]{:S(2)}) copy-start(bf16[512,1024]{1,0:T(8,128)(2,1)} %param.6) | copy-start | bytes 3145732
  8.4 4.7 %copy-start.3 = (bf16[1024,1408]{1,0:T(8,128)(2,1)S(1)}, bf16[1024,1408]{1,0:T(8,128)(2,1)}, u32[]{:S(2)}) copy-start(bf16[1024,1408]{1,0:T(8,128)(2,1)} %param.8) | copy-start | bytes 8650756
  16.6 189.6 %reduce-scatter.2.cloned.1.call-start = ((), (), s32[]{:S(2)}) async-start(), calls=%async_computation.1 | async-start | bytes 2359296 | tf_op jit(solution)/shard_map/reduce_scatter | solution.py:22
  137.4 2.9 %copy-start.2 = (bf16[1024]{0:T(1024)(128)(2,1)S(1)}, bf16[1024]{0:T(1024)(128)(2,1)}, u32[]{:S(2)}) copy-start(bf16[1024]{0:T(1024)(128)(2,1)} %param.11) | copy-start | bytes 6148
Sparse Core Ops, SparseCore 0:
  16.7 113.7 all-reduce.2
  137.5 68.6 reduce-scatter.1
where the time goes:
time: 222 us
  waiting for transfers between devices  170 us (77%)
  matrix products  15 us (7%)
  blocking collectives  14 us (6%)
  between operations  13.4 us (6%)
  other arithmetic  8.13 us (4%)
    psum x1, waiting for transfers between devices, body(): total_sq, gate_sum, up_sum = lax.psum((local_sq, gate_part, up_part), 'cb')  104 us
    reduce_scatter x1, waiting for transfers between devices, body(): down = lax.psum_scatter(partial_down, 'ra', scatter_dimension=0, tiled=True)  66 us
    psum x1, blocking collectives, body(): total_sq, gate_sum, up_sum = lax.psum((local_sq, gate_part, up_part), 'cb')  8.37 us
    dot_general x1, matrix products, body(): partial_down = jnp.dot(hidden, w_down, preferred_element_type=jnp.float32)  6.83 us
    psum x1, blocking collectives, body(): out_sq = lax.psum(jnp.sum(mixed * mixed, axis=1), 'cb')  5.67 us
    dot_general x1, matrix products, body(): up_part = jnp.dot(scaled, w_up, preferred_element_type=jnp.float32)  4.74 us
  transfers between devices with their start and end apart: 2, of which 2 were waited for; matrix products, arithmetic and copies ran while one was open for 2% of the time, Pallas kernels for 0%

commit v1 on v0

v1 whole, which is shorter than its diff:
```python
import functools

import jax
import jax.numpy as jnp
from jax import lax
from jax.experimental import pallas as pl
from jax.experimental.pallas import tpu as pltpu
from jax.sharding import PartitionSpec as P

EPS = 1e-06
LANES = 128
TILE = 256
CHUNKS = 4
VMEM_BYTES = 64 * 1024 * 1024 - 64 * 1024


def plain_body(width, tokens, norm_gain, w_gate, w_up, w_down, out_gain):
    xfloat = tokens.astype(jnp.float32)
    local_sq = jnp.sum(xfloat * xfloat, axis=1)
    scaled = (xfloat * norm_gain.astype(jnp.float32)).astype(jnp.bfloat16)
    gate_part = jnp.dot(scaled, w_gate, preferred_element_type=jnp.float32)
    up_part = jnp.dot(scaled, w_up, preferred_element_type=jnp.float32)
    total_sq, gate_sum, up_sum = lax.psum((local_sq, gate_part, up_part), "cb")
    inv_in = lax.rsqrt(total_sq / width + EPS)[:, None]
    hidden = (jax.nn.silu(gate_sum * inv_in) * (up_sum * inv_in)).astype(jnp.bfloat16)
    partial_down = jnp.dot(hidden, w_down, preferred_element_type=jnp.float32)
    own_rows = tokens.shape[0] // lax.axis_size("ra")
    first_row = lax.axis_index("ra") * own_rows
    down = lax.psum_scatter(partial_down, "ra", scatter_dimension=0, tiled=True)
    residual = lax.dynamic_slice_in_dim(xfloat, first_row, own_rows, 0)
    mixed = 0.1 * residual + down
    out_sq = lax.psum(jnp.sum(mixed * mixed, axis=1), "cb")
    inv_out = lax.rsqrt(out_sq / width + EPS)[:, None]
    return (mixed * inv_out * out_gain.astype(jnp.float32)).astype(jnp.bfloat16)


def kernel(n_ra, width, tok_hbm, ng_hbm, wg_hbm, wu_hbm, wd_hbm, og_hbm, out_ref,
           tok, rest, ng, og, wgu, wd, xs, xb, mixed,
           part, prec, xrec, sqp, sqd, sqx, hid, dn, yrec, zrec, osq,
           ld, s_d, r_d, s_x, r_x, s_hx, r_hx, s_h1, r_h1, s_h2, r_h2,
           s_y, r_y, s_z, r_z, s_o, r_o, s_q, r_q):
    chunks, rows, depth = xs.shape
    units = wd.shape[0]
    own = rest.shape[0]
    sub = own // chunks
    nz = n_ra // 2
    quarter = rows // 4
    ra, cb = lax.axis_index("ra"), lax.axis_index("cb")
    c, x = lax.rem(cb, 2), lax.div(cb, 2)
    y, z = lax.rem(ra, 2), lax.div(ra, 2)
    oc, ox, oy = 1 - c, 1 - x, 1 - y
    core_peer = (ra, x * 2 + oc)
    x_peer = (ra, ox * 2 + c)
    diag_peer = (ra, ox * 2 + oc)
    y_peer = (z * 2 + oy, cb)
    z_peers = [(lax.rem(z + d, nz) * 2 + y, cb) for d in range(1, nz)]
    mesh_id = pl.DeviceIdType.MESH

    loads = [
        pltpu.make_async_copy(tok_hbm, tok, ld.at[0]),
        pltpu.make_async_copy(ng_hbm, ng, ld.at[1]),
        pltpu.make_async_copy(wg_hbm, wgu.at[:, pl.ds(0, units)], ld.at[2]),
        pltpu.make_async_copy(wu_hbm, wgu.at[:, pl.ds(units, units)], ld.at[3]),
        pltpu.make_async_copy(tok_hbm.at[pl.ds(pl.multiple_of(ra * own, own), own)], rest, ld.at[4]),
        pltpu.make_async_copy(og_hbm, og, ld.at[5]),
        pltpu.make_async_copy(wd_hbm, wd, ld.at[6]),
    ]
    for load in loads:
        load.start()

    barrier = pltpu.get_barrier_semaphore()
    peers = [core_peer, x_peer, diag_peer, y_peer] + z_peers
    for peer in peers:
        pl.semaphore_signal(barrier, inc=1, device_id=peer, device_id_type=mesh_id)

    sends = []

    def send(src, dst, s, r, peer):
        copy = pltpu.make_async_remote_copy(
            src_ref=src, dst_ref=dst, send_sem=s, recv_sem=r,
            device_id=peer, device_id_type=mesh_id)
        copy.start()
        sends.append(copy)
        return copy

    loads[0].wait()
    loads[1].wait()
    lane = lax.broadcasted_iota(jnp.int32, (sub, LANES), 1)
    gain = ng[...].astype(jnp.float32)
    for d in range(n_ra):
        xf = tok[pl.ds(d * own, own), :].astype(jnp.float32)
        sq = jnp.sum(xf * xf, axis=1, keepdims=True)
        sc = xf * gain
        at = (d % 2) * nz * sub + (d // 2) * sub
        total = jnp.zeros((sub, LANES), jnp.float32)
        for k in range(chunks):
            xs[k, pl.ds(at, sub), :] = sc[k * sub:(k + 1) * sub]
            total = total + jnp.where(lane == k, sq[k * sub:(k + 1) * sub], 0.0)
        q, off = at // quarter, at % quarter
        sqp[q // 2, q % 2, pl.ds(off, sub), :] = total
    for k in range(chunks):
        xb[k] = xs[k].astype(jnp.bfloat16)

    def project(k):
        def tile(j, carry):
            cols = pl.ds(pl.multiple_of(j * TILE, TILE), TILE)
            got = jnp.dot(xb[k], wgu[:, cols], preferred_element_type=jnp.float32)
            part[k, :, :, :, cols] = got.reshape(2, 2, quarter, TILE)
            return carry
        lax.fori_loop(0, 2 * units // TILE, tile, 0)
        return send(part.at[k, oc], prec.at[k], s_d.at[k], r_d.at[k], core_peer)

    def combine(k, copy):
        copy.wait_recv()
        def tile(j, carry):
            cols = pl.ds(pl.multiple_of(j * TILE, TILE), TILE)
            part[k, c, :, :, cols] += prec[k, :, :, cols]
            return carry
        lax.fori_loop(0, 2 * units // TILE, tile, 0)
        return send(part.at[k, c, ox], xrec.at[k], s_x.at[k], r_x.at[k], x_peer)

    def activate(k, copy, inv):
        copy.wait_recv()
        scale = inv[:, k:k + 1]
        def tile(j, carry):
            left = pl.ds(pl.multiple_of(j * LANES, LANES), LANES)
            right = pl.ds(pl.multiple_of(units + j * LANES, LANES), LANES)
            gate = (part[k, c, x, :, left] + xrec[k, :, left]) * scale
            up = (part[k, c, x, :, right] + xrec[k, :, right]) * scale
            val = gate / (1.0 + jnp.exp(-gate)) * up
            hid[k, c, x, :, left] = val.astype(jnp.bfloat16).astype(jnp.float32)
            return carry
        lax.fori_loop(0, units // LANES, tile, 0)
        block = hid.at[k, c, x]
        hx = send(block, block, s_hx.at[k], r_hx.at[k], x_peer)
        h1 = send(block, block, s_h1.at[k], r_h1.at[k], core_peer)
        return hx, h1

    def forward(k, hx):
        hx.wait_recv()
        block = hid.at[k, c, ox]
        return send(block, block, s_h2.at[k], r_h2.at[k], core_peer)

    def lower(k, h1, h2):
        h1.wait_recv()
        h2.wait_recv()
        hb = hid[k].reshape(rows, units).astype(jnp.bfloat16)
        for j in range(depth // TILE):
            cols = slice(j * TILE, (j + 1) * TILE)
            got = jnp.dot(hb, wd[:, cols], preferred_element_type=jnp.float32)
            dn[k, :, :, :, cols] = got.reshape(2, nz, sub, TILE)
        return send(dn.at[k, oy], yrec.at[k], s_y.at[k], r_y.at[k], y_peer)

    def across(k, copy):
        copy.wait_recv()
        dn[k, y] += yrec[k]
        return [
            send(dn.at[k, y, lax.rem(z + d, nz)], zrec.at[k, d - 1],
                 s_z.at[k, d - 1], r_z.at[k, d - 1], z_peers[d - 1])
            for d in range(1, nz)]

    def finish(k, copies):
        got = dn[k, y, z]
        for d, copy in enumerate(copies):
            copy.wait_recv()
            got = got + zrec[k, d]
        got = 0.1 * rest[pl.ds(k * sub, sub), :].astype(jnp.float32) + got
        mixed[pl.ds(k * sub, sub), :] = got
        osq[0, k] = jnp.broadcast_to(jnp.sum(got * got, axis=1, keepdims=True), (sub, LANES))
        return [
            send(osq.at[0, k], osq.at[i + 1, k], s_o.at[k, i], r_o.at[k, i], peer)
            for i, peer in enumerate((core_peer, x_peer, diag_peer))]

    pl.semaphore_wait(barrier, len(peers))
    q1 = send(sqp.at[oc], sqd, s_q.at[0], r_q.at[0], core_peer)
    loads[2].wait()
    loads[3].wait()
    a, b, h1, h2, hx, ys, zs, os = {}, {}, {}, {}, {}, {}, {}, {}
    a[0] = project(0)
    q1.wait_recv()
    sqp[c] += sqd[...]
    q2 = send(sqp.at[c, ox], sqx, s_q.at[1], r_q.at[1], x_peer)
    if chunks > 1:
        a[1] = project(1)
    for k in range(min(2, chunks)):
        b[k] = combine(k, a[k])
    q2.wait_recv()
    inv = lax.rsqrt((sqp[c, x] + sqx[...]) / width + EPS)
    loads[4].wait()
    loads[5].wait()
    for t in range(chunks + 3):
        if t + 2 < chunks:
            a[t + 2] = project(t + 2)
        if t < chunks:
            hx[t], h1[t] = activate(t, b[t], inv)
        if t + 2 < chunks:
            b[t + 2] = combine(t + 2, a[t + 2])
        if 0 <= t - 1 < chunks:
            if t == 1:
                loads[6].wait()
            h2[t - 1] = forward(t - 1, hx[t - 1])
            ys[t - 1] = lower(t - 1, h1[t - 1], h2[t - 1])
        if 0 <= t - 2 < chunks:
            zs[t - 2] = across(t - 2, ys[t - 2])
        if 0 <= t - 3 < chunks:
            os[t - 3] = finish(t - 3, zs[t - 3])
    for k in range(chunks):
        for copy in os[k]:
            copy.wait_recv()
    osum = osq[0] + osq[1] + osq[2] + osq[3]
    inv_out = lax.rsqrt(osum.reshape(own, LANES) / width + EPS)[:, :1]
    out_ref[...] = (mixed[...] * inv_out * og[...].astype(jnp.float32)).astype(out_ref.dtype)
    for copy in sends:
        copy.wait_send()


def fused_body(n_ra, width, tokens, norm_gain, w_gate, w_up, w_down, out_gain):
    count, depth = tokens.shape
    units = w_down.shape[0]
    own = count // n_ra
    rows, sub, quarter = count // CHUNKS, own // CHUNKS, count // CHUNKS // 4
    nz = n_ra // 2
    f32, bf16 = jnp.float32, jnp.bfloat16
    dma = pltpu.SemaphoreType.DMA
    per = [dma((CHUNKS,)) for _ in range(12)]
    return pl.pallas_call(
        functools.partial(kernel, n_ra, width),
        out_shape=jax.ShapeDtypeStruct((own, depth), bf16),
        in_specs=[pl.BlockSpec(memory_space=pl.ANY)] * 6,
        out_specs=pl.BlockSpec(memory_space=pltpu.VMEM),
        scratch_shapes=[
            pltpu.VMEM((count, depth), bf16),
            pltpu.VMEM((own, depth), bf16),
            pltpu.VMEM((1, depth), bf16),
            pltpu.VMEM((1, depth), bf16),
            pltpu.VMEM((depth, 2 * units), bf16),
            pltpu.VMEM((units, depth), bf16),
            pltpu.VMEM((CHUNKS, rows, depth), f32),
            pltpu.VMEM((CHUNKS, rows, depth), bf16),
            pltpu.VMEM((own, depth), f32),
            pltpu.VMEM((CHUNKS, 2, 2, quarter, 2 * units), f32),
            pltpu.VMEM((CHUNKS, 2, quarter, 2 * units), f32),
            pltpu.VMEM((CHUNKS, quarter, 2 * units), f32),
            pltpu.VMEM((2, 2, quarter, LANES), f32),
            pltpu.VMEM((2, quarter, LANES), f32),
            pltpu.VMEM((quarter, LANES), f32),
            pltpu.VMEM((CHUNKS, 2, 2, quarter, units), f32),
            pltpu.VMEM((CHUNKS, 2, nz, sub, depth), f32),
            pltpu.VMEM((CHUNKS, nz, sub, depth), f32),
            pltpu.VMEM((CHUNKS, nz - 1, sub, depth), f32),
            pltpu.VMEM((4, CHUNKS, sub, LANES), f32),
            dma((7,)),
            *per,
            dma((CHUNKS, nz - 1)),
            dma((CHUNKS, nz - 1)),
            dma((CHUNKS, 3)),
            dma((CHUNKS, 3)),
            dma((2,)),
            dma((2,)),
        ],
        compiler_params=pltpu.CompilerParams(
            collective_id=0, has_side_effects=True, vmem_limit_bytes=VMEM_BYTES),
    )(tokens, norm_gain.reshape(1, depth), w_gate, w_up, w_down, out_gain.reshape(1, depth))


def solution(mesh):
    n_ra, n_cb = mesh.shape["ra"], mesh.shape["cb"]

    def body(*args):
        tokens, w_down = args[0], args[4]
        count, depth = tokens.shape
        units = w_down.shape[0]
        width = depth * n_cb
        tiled = (
            n_cb == 4 and n_ra % 2 == 0 and n_ra > 2
            and count % (n_ra * CHUNKS * 8) == 0 and units % LANES == 0 and depth % TILE == 0
            and (count // CHUNKS // 4) % (count // n_ra // CHUNKS) == 0)
        if tiled:
            return fused_body(n_ra, width, *args)
        return plain_body(width, *args)

    return jax.shard_map(
        body,
        mesh=mesh,
        in_specs=(P(None, "cb"), P("cb"), P("cb", "ra"), P("cb", "ra"), P("ra", "cb"), P("cb")),
        out_specs=P("ra", "cb"),
        check_vma=False,
    )
```

time: 222 us -> 86.2 us (0.39)
  waiting for transfers between devices: 170 us -> 0 us
  Pallas kernels: 0 us -> 81.9 us
  matrix products: 15 us -> 0 us
  blocking collectives: 14 us -> 0 us
  between operations: 13.4 us -> 0.01 us
  other arithmetic: 8.13 us -> 0 us
  local copies, waits for them, and re-layouts: 1.01 us -> 4.12 us
    psum x1 -> x0, waiting for transfers between devices: 104 us -> none  [body(): total_sq, gate_sum, up_sum = lax.psum((local_sq, gate_part, up_part), 'cb')]
    pallas_call x0 -> x1, Pallas kernels: none -> 81.9 us  [fused_body(): pl.pallas_call(functools.partial(kernel, n_ra, width), out_shape=jax.Shap...]
    reduce_scatter x1 -> x0, waiting for transfers between devices: 66 us -> none  [body(): down = lax.psum_scatter(partial_down, 'ra', scatter_dimension=0, tiled=True)]
    dot_general x3 -> x0, matrix products: 15 us -> none  [the longest x1 6.83 us: body(): partial_down = jnp.dot(hidden, w_down, preferred_element_type=jnp.float32)]
    psum x2 -> x0, blocking collectives: 14 us -> none  [the longest x1 8.37 us: body(): total_sq, gate_sum, up_sum = lax.psum((local_sq, gate_part, up_part), 'cb')]
    convert_element_type x4 -> x0, other arithmetic: 5.44 us -> none  [the longest x1 2.82 us: body(): xfloat = tokens.astype(jnp.float32)]
    reduce_sum x2 -> x0, other arithmetic: 2.67 us -> none  [the longest x1 1.5 us: body(): local_sq = jnp.sum(xfloat * xfloat, axis=1)]
    reshape x0 -> x2, local copies, waits for them, and re-layouts: none -> 2.55 us  [the longest x1 1.28 us: fused_body(): norm_gain.reshape(1, depth)]
  transfers between devices with their start and end apart: 2 -> 0, of which waited for: 2 -> 0; matrix products, arithmetic and copies ran while one was open for 2% -> 0% of each run, Pallas kernels for 0% -> 0%
where the time goes in v1:
time: 86.2 us; the launch traced here: 86.1 us
  Pallas kernels  81.9 us (95%)
  local copies, waits for them, and re-layouts  4.12 us (5%)
    pallas_call x1, Pallas kernels, fused_body(): pl.pallas_call(functools.partial(kernel, n_ra, width), out_shape=jax.Shap...  81.9 us

profile of v1, /device:TPU:0, one launch (start us, length us, event | category | flops | bytes accessed | tf_op | source)
XLA Modules:
  0.0 86.1 jit_solution(10991648414074429167)
XLA Ops:
  0.0 1.3 %reshape.6.ng_hbm = bf16[1,1024]{1,0:T(2,128)(2,1)} reshape(bf16[1024]{0:T(1024)(128)(2,1)} %param.7) | data formatting | bytes 4096 | tf_op jit(solution)/shard_map/reshape | solution.py:263
  1.3 1.3 %reshape.7.og_hbm = bf16[1,1024]{1,0:T(2,128)(2,1)} reshape(bf16[1024]{0:T(1024)(128)(2,1)} %param.11) | data formatting | bytes 4096 | tf_op jit(solution)/shard_map/reshape | solution.py:263
  2.5 81.9 %shard_map.64 = bf16[64,1024]{1,0:T(8,128)(2,1)} custom-call(bf16[512,1024]{1,0:T(8,128)(2,1)} %tok_hbm.1, bf16[1,1024]{1,0:T(2,128)(2,1)} %reshape.6.ng_hbm, bf16[1024,1408]{1,0:T(8,128)(2,1)} %wg_hbm.1, bf16[1024,1408]{1,0:T(8,128)(2,1)} %wu_hbm.1, bf16[1408,1024]{1,0:T(8,128)(2,1)} %wd_hbm.1, bf16[1,1024]{1,0:T(2,128)(2,1)} %reshape.7.og_hbm), custom_call_target="tpu_custom_call" | custom-call | tf_op jit(solution)/shard_map/pallas_call | solution.py:226
  84.5 1.6 %copy.8 = bf16[64,1024]{1,0:T(8,128)(2,1)} copy(bf16[64,1024]{1,0:T(8,128)(2,1)} %shard_map.64) | data formatting | bytes 262144

commit v2 on v0

v2 whole, which is shorter than its diff:
```python
import functools

import jax
import jax.numpy as jnp
from jax import lax
from jax.experimental import pallas as pl
from jax.experimental.pallas import tpu as pltpu
from jax.sharding import PartitionSpec as P

EPS = 1e-06
LANES = 128
TILE = 256
PIECES = 3
SHARES = (1, 2, 2, 1, 1, 1)
UNITS = sum(SHARES)
VMEM_BYTES = 64 * 1024 * 1024 - 64 * 1024


def plain_body(width, tokens, norm_gain, w_gate, w_up, w_down, out_gain):
    xfloat = tokens.astype(jnp.float32)
    local_sq = jnp.sum(xfloat * xfloat, axis=1)
    scaled = (xfloat * norm_gain.astype(jnp.float32)).astype(jnp.bfloat16)
    gate_part = jnp.dot(scaled, w_gate, preferred_element_type=jnp.float32)
    up_part = jnp.dot(scaled, w_up, preferred_element_type=jnp.float32)
    total_sq, gate_sum, up_sum = lax.psum((local_sq, gate_part, up_part), "cb")
    inv_in = lax.rsqrt(total_sq / width + EPS)[:, None]
    hidden = (jax.nn.silu(gate_sum * inv_in) * (up_sum * inv_in)).astype(jnp.bfloat16)
    partial_down = jnp.dot(hidden, w_down, preferred_element_type=jnp.float32)
    own_rows = tokens.shape[0] // lax.axis_size("ra")
    first_row = lax.axis_index("ra") * own_rows
    down = lax.psum_scatter(partial_down, "ra", scatter_dimension=0, tiled=True)
    residual = lax.dynamic_slice_in_dim(xfloat, first_row, own_rows, 0)
    mixed = 0.1 * residual + down
    out_sq = lax.psum(jnp.sum(mixed * mixed, axis=1), "cb")
    inv_out = lax.rsqrt(out_sq / width + EPS)[:, None]
    return (mixed * inv_out * out_gain.astype(jnp.float32)).astype(jnp.bfloat16)


def kernel(n_ra, width, subs, *refs):
    it = iter(refs)

    def take(count):
        return [next(it) for _ in range(count)]

    n = len(subs)
    tok_hbm, ng_hbm, wg_hbm, wu_hbm, wd_hbm, og_hbm, out_ref = take(7)
    tok, rest, ng, og, wgu, wd, xs, mixed, sqp, sqd, sqx, osq = take(12)
    xb, part, prec, xrec, hid, dn, yrec, zrec = [take(n) for _ in range(8)]
    ld, lw, s_d, r_d, s_x, r_x, s_h, r_h, s_y, r_y, s_z, r_z, s_o, r_o, s_q, r_q = take(16)
    depth, units = xs.shape[1], wd.shape[0]
    own = rest.shape[0]
    base = [sum(subs[:k]) for k in range(n)]
    nz = n_ra // 2
    ra, cb = lax.axis_index("ra"), lax.axis_index("cb")
    c, x = lax.rem(cb, 2), lax.div(cb, 2)
    y, z = lax.rem(ra, 2), lax.div(ra, 2)
    oc, ox, oy = 1 - c, 1 - x, 1 - y
    core_peer = (ra, x * 2 + oc)
    x_peer = (ra, ox * 2 + c)
    diag_peer = (ra, ox * 2 + oc)
    y_peer = (z * 2 + oy, cb)
    z_peers = [(lax.rem(z + d, nz) * 2 + y, cb) for d in range(1, nz)]
    mesh_id = pl.DeviceIdType.MESH
    pieces = column_pieces(2 * units)
    halves = [(0, depth // 2), (depth // 2, depth // 2)]

    early = [
        pltpu.make_async_copy(tok_hbm, tok, ld.at[0]),
        pltpu.make_async_copy(ng_hbm, ng, ld.at[1]),
    ]
    weights = []
    for p, (start, size) in enumerate(pieces):
        got = []
        for i, (ref, low) in enumerate(((wg_hbm, 0), (wu_hbm, units))):
            lo, hi = max(start, low), min(start + size, low + units)
            if lo < hi:
                got.append(pltpu.make_async_copy(
                    ref.at[:, pl.ds(lo - low, hi - lo)], wgu.at[:, pl.ds(lo, hi - lo)], lw.at[p, i]))
        weights.append(got)
    late = [
        pltpu.make_async_copy(tok_hbm.at[pl.ds(pl.multiple_of(ra * own, own), own)], rest, ld.at[2]),
        pltpu.make_async_copy(og_hbm, og, ld.at[3]),
        pltpu.make_async_copy(wd_hbm, wd, ld.at[4]),
    ]
    for load in early + sum(weights, []) + late:
        load.start()

    barrier = pltpu.get_barrier_semaphore()
    peers = [core_peer, x_peer, diag_peer, y_peer] + z_peers
    for peer in peers:
        pl.semaphore_signal(barrier, inc=1, device_id=peer, device_id_type=mesh_id)

    sends = []

    def send(src, dst, s, r, peer):
        copy = pltpu.make_async_remote_copy(
            src_ref=src, dst_ref=dst, send_sem=s, recv_sem=r,
            device_id=peer, device_id_type=mesh_id)
        copy.start()
        sends.append(copy)
        return copy

    def project(k, p):
        with jax.named_scope(f"project{k}"):
            start, size = pieces[p]
            cols = pl.ds(start, size)
            got = jnp.dot(xb[k][...], wgu[:, cols], preferred_element_type=jnp.float32)
            part[k][:, :, :, cols] = got.reshape(2, 2, part[k].shape[2], size)

    def to_core(k, cols, p):
        return send(part[k].at[oc, :, :, cols], prec[k].at[:, :, cols], s_d.at[k, p], r_d.at[k, p], core_peer)

    def combine(k, copy, start, size, p):
        with jax.named_scope(f"combine{k}"):
            copy.wait_recv()
            cols = pl.ds(start, size)
            part[k][c, :, :, cols] += prec[k][:, :, cols]
            return send(part[k].at[c, ox, :, cols], xrec[k].at[:, cols], s_x.at[k, p], r_x.at[k, p], x_peer)

    def whole(k):
        for p in range(len(pieces)):
            project(k, p)
        return to_core(k, pl.ds(0, 2 * units), 0)

    def join(k, copy):
        return [combine(k, copy, 0, 2 * units, 0)]

    def activate(k, copies, inv):
        with jax.named_scope(f"activate{k}"):
            for copy in copies:
                copy.wait_recv()
            scale = inv[:part[k].shape[2], k:k + 1]
            gate = (part[k][c, x, :, :units] + xrec[k][:, :units]) * scale
            up = (part[k][c, x, :, units:] + xrec[k][:, units:]) * scale
            val = gate / (1.0 + jnp.exp(-gate)) * up
            hid[k][c, x] = val.astype(jnp.bfloat16).astype(jnp.float32)
            block = hid[k].at[c, x]
            hx = send(block, block, s_h.at[k, 0], r_h.at[k, 0], x_peer)
            h1 = send(block, block, s_h.at[k, 1], r_h.at[k, 1], core_peer)
            return hx, h1

    def forward(k, hx):
        with jax.named_scope(f"forward{k}"):
            hx.wait_recv()
            block = hid[k].at[c, ox]
            return send(block, block, s_h.at[k, 2], r_h.at[k, 2], core_peer)

    def lower(k, h1, h2):
        with jax.named_scope(f"lower{k}"):
            h1.wait_recv()
            h2.wait_recv()
            hb = hid[k][...].reshape(n_ra * subs[k], units).astype(jnp.bfloat16)
            out = []
            for h, (start, size) in enumerate(halves):
                cols = pl.ds(start, size)
                got = jnp.dot(hb, wd[:, cols], preferred_element_type=jnp.float32)
                dn[k][:, :, :, cols] = got.reshape(2, nz, subs[k], size)
                out.append(send(dn[k].at[oy, :, :, cols], yrec[k].at[:, :, cols],
                                s_y.at[k, h], r_y.at[k, h], y_peer))
            return out

    def across(k, copies):
        with jax.named_scope(f"across{k}"):
            out = []
            for h, (start, size) in enumerate(halves):
                cols = pl.ds(start, size)
                copies[h].wait_recv()
                dn[k][y, :, :, cols] += yrec[k][:, :, cols]
                for d in range(1, nz):
                    out.append(send(
                        dn[k].at[y, lax.rem(z + d, nz), :, cols], zrec[k].at[d - 1, :, cols],
                        s_z.at[k, h, d - 1], r_z.at[k, h, d - 1], z_peers[d - 1]))
            return out

    def finish(k, copies):
        with jax.named_scope(f"finish{k}"):
            for copy in copies:
                copy.wait_recv()
            got = dn[k][y, z]
            for d in range(nz - 1):
                got = got + zrec[k][d]
            at = pl.ds(base[k], subs[k])
            got = mixed[at, :] + got
            mixed[at, :] = got
            osq[0, at, :] = jnp.broadcast_to(jnp.sum(got * got, axis=1, keepdims=True), (subs[k], LANES))
            return [
                send(osq.at[0, at], osq.at[i + 1, at], s_o.at[k, i], r_o.at[k, i], peer)
                for i, peer in enumerate((core_peer, x_peer, diag_peer))]

    def fill(k):
        xb[k][...] = jnp.concatenate(
            [xs[pl.ds((zz * 2 + yy) * own + base[k], subs[k]), :] for yy in range(2) for zz in range(nz)],
            axis=0).astype(jnp.bfloat16)

    with jax.named_scope("tokens"):
        for load in early:
            load.wait()
    with jax.named_scope("scale"):
        gain = ng[...].astype(jnp.float32)
        for d in range(n_ra):
            at = pl.ds(d * own, own)
            xs[at, :] = tok[at, :].astype(jnp.float32) * gain
        fill(0)
    with jax.named_scope("enter"):
        pl.semaphore_wait(barrier, len(peers))

    a, b, h1, h2, hx, ys, zs, os = {}, {}, {}, {}, {}, {}, {}, {}
    heads, b[0] = [], []
    for p, (start, size) in enumerate(pieces):
        with jax.named_scope("weights"):
            for load in weights[p]:
                load.wait()
        project(0, p)
        heads.append(to_core(0, pl.ds(start, size), p))
        if p > 0:
            b[0].append(combine(0, heads[p - 1], *pieces[p - 1], p - 1))
    with jax.named_scope("squares"):
        lane = lax.broadcasted_iota(jnp.int32, (own, LANES), 1)
        sqp[...] = jnp.zeros_like(sqp)
        for d in range(n_ra):
            xf = tok[pl.ds(d * own, own), :].astype(jnp.float32)
            sq = jnp.broadcast_to(jnp.sum(xf * xf, axis=1, keepdims=True), (own, LANES))
            for k in range(n):
                at = ((d % 2) * nz + d // 2) * subs[k]
                quarter = nz * subs[k] // 2
                q, off = at // quarter, at % quarter
                val = jnp.where(lane[:subs[k]] == k, sq[base[k]:base[k] + subs[k]], 0.0)
                sqp[q // 2, q % 2, pl.ds(off, subs[k]), :] += val
        q1 = send(sqp.at[oc], sqd, s_q.at[0], r_q.at[0], core_peer)
    last = len(pieces) - 1
    b[0].append(combine(0, heads[last], *pieces[last], last))
    fill(1)
    a[1] = whole(1)
    q1.wait_recv()
    sqp[c] += sqd[...]
    q2 = send(sqp.at[c, ox], sqx, s_q.at[1], r_q.at[1], x_peer)
    b[1] = join(1, a[1])
    for k in range(2, n):
        fill(k)
    for load in late:
        load.wait()
    mixed[...] = 0.1 * rest[...].astype(jnp.float32)
    for t in range(n + 3):
        if t + 2 < n:
            a[t + 2] = whole(t + 2)
        if t == 0:
            q2.wait_recv()
            inv = lax.rsqrt((sqp[c, x] + sqx[...]) / width + EPS)
        if t < n:
            hx[t], h1[t] = activate(t, b[t], inv)
        if t + 2 < n:
            b[t + 2] = join(t + 2, a[t + 2])
        if 0 <= t - 1 < n:
            h2[t - 1] = forward(t - 1, hx[t - 1])
            ys[t - 1] = lower(t - 1, h1[t - 1], h2[t - 1])
        if 0 <= t - 2 < n:
            zs[t - 2] = across(t - 2, ys[t - 2])
        if 0 <= t - 3 < n:
            os[t - 3] = finish(t - 3, zs[t - 3])
    with jax.named_scope("norm"):
        for k in range(n):
            for copy in os[k]:
                copy.wait_recv()
        osum = osq[0] + osq[1] + osq[2] + osq[3]
        inv_out = lax.rsqrt(osum / width + EPS)[:, :1]
        out_ref[...] = (mixed[...] * inv_out * og[...].astype(jnp.float32)).astype(out_ref.dtype)
    with jax.named_scope("drain"):
        for copy in sends:
            copy.wait_send()


def column_pieces(total):
    tiles = total // TILE
    cuts = [tiles * i // PIECES * TILE for i in range(PIECES)] + [total]
    return [(lo, hi - lo) for lo, hi in zip(cuts[:-1], cuts[1:])]


def chunk_rows(own):
    unit = own // UNITS
    return [unit * share for share in SHARES]


def fused_body(n_ra, width, tokens, norm_gain, w_gate, w_up, w_down, out_gain):
    count, depth = tokens.shape
    units = w_down.shape[0]
    own = count // n_ra
    subs = chunk_rows(own)
    n, nz = len(subs), n_ra // 2
    f32, bf16 = jnp.float32, jnp.bfloat16
    dma = pltpu.SemaphoreType.DMA
    quarters = [n_ra * sub // 4 for sub in subs]
    most = max(quarters)
    return pl.pallas_call(
        functools.partial(kernel, n_ra, width, subs),
        out_shape=jax.ShapeDtypeStruct((own, depth), bf16),
        in_specs=[pl.BlockSpec(memory_space=pl.ANY)] * 6,
        out_specs=pl.BlockSpec(memory_space=pltpu.VMEM),
        scratch_shapes=[
            pltpu.VMEM((count, depth), bf16),
            pltpu.VMEM((own, depth), bf16),
            pltpu.VMEM((1, depth), bf16),
            pltpu.VMEM((1, depth), bf16),
            pltpu.VMEM((depth, 2 * units), bf16),
            pltpu.VMEM((units, depth), bf16),
            pltpu.VMEM((count, depth), f32),
            pltpu.VMEM((own, depth), f32),
            pltpu.VMEM((2, 2, most, LANES), f32),
            pltpu.VMEM((2, most, LANES), f32),
            pltpu.VMEM((most, LANES), f32),
            pltpu.VMEM((4, own, LANES), f32),
            *[pltpu.VMEM((n_ra * sub, depth), bf16) for sub in subs],
            *[pltpu.VMEM((2, 2, quarter, 2 * units), f32) for quarter in quarters],
            *[pltpu.VMEM((2, quarter, 2 * units), f32) for quarter in quarters],
            *[pltpu.VMEM((quarter, 2 * units), f32) for quarter in quarters],
            *[pltpu.VMEM((2, 2, quarter, units), f32) for quarter in quarters],
            *[pltpu.VMEM((2, nz, sub, depth), f32) for sub in subs],
            *[pltpu.VMEM((nz, sub, depth), f32) for sub in subs],
            *[pltpu.VMEM((nz - 1, sub, depth), f32) for sub in subs],
            dma((5,)),
            dma((PIECES, 2)),
            *[dma((n, PIECES)) for _ in range(4)],
            *[dma((n, 3)) for _ in range(2)],
            *[dma((n, 2)) for _ in range(2)],
            *[dma((n, 2, nz - 1)) for _ in range(2)],
            *[dma((n, 3)) for _ in range(2)],
            *[dma((2,)) for _ in range(2)],
        ],
        compiler_params=pltpu.CompilerParams(
            collective_id=0, has_side_effects=True, vmem_limit_bytes=VMEM_BYTES),
    )(tokens, norm_gain.reshape(1, depth), w_gate, w_up, w_down, out_gain.reshape(1, depth))


def solution(mesh):
    n_ra, n_cb = mesh.shape["ra"], mesh.shape["cb"]

    def body(*args):
        tokens, w_down = args[0], args[4]
        count, depth = tokens.shape
        units = w_down.shape[0]
        width = depth * n_cb
        tiled = (
            n_cb == 4 and n_ra % 4 == 0 and n_ra > 2
            and count % (n_ra * UNITS * 8) == 0 and units % LANES == 0 and depth % TILE == 0)
        if tiled:
            return fused_body(n_ra, width, *args)
        return plain_body(width, *args)

    return jax.shard_map(
        body,
        mesh=mesh,
        in_specs=(P(None, "cb"), P("cb"), P("cb", "ra"), P("cb", "ra"), P("ra", "cb"), P("cb")),
        out_specs=P("ra", "cb"),
        check_vma=False,
    )
```

time: 222 us -> 77.2 us (0.35)
  waiting for transfers between devices: 170 us -> 0 us
  Pallas kernels: 0 us -> 72.9 us
  matrix products: 15 us -> 0 us
  blocking collectives: 14 us -> 0 us
  between operations: 13.4 us -> 0.01 us
  other arithmetic: 8.13 us -> 0 us
  local copies, waits for them, and re-layouts: 1.01 us -> 4.12 us
    psum x1 -> x0, waiting for transfers between devices: 104 us -> none  [body(): total_sq, gate_sum, up_sum = lax.psum((local_sq, gate_part, up_part), 'cb')]
    pallas_call x0 -> x1, Pallas kernels: none -> 72.9 us  [fused_body(): pl.pallas_call(functools.partial(kernel, n_ra, width, subs), out_shape=ja...]
    reduce_scatter x1 -> x0, waiting for transfers between devices: 66 us -> none  [body(): down = lax.psum_scatter(partial_down, 'ra', scatter_dimension=0, tiled=True)]
    dot_general x3 -> x0, matrix products: 15 us -> none  [the longest x1 6.83 us: body(): partial_down = jnp.dot(hidden, w_down, preferred_element_type=jnp.float32)]
    psum x2 -> x0, blocking collectives: 14 us -> none  [the longest x1 8.37 us: body(): total_sq, gate_sum, up_sum = lax.psum((local_sq, gate_part, up_part), 'cb')]
    convert_element_type x4 -> x0, other arithmetic: 5.44 us -> none  [the longest x1 2.82 us: body(): xfloat = tokens.astype(jnp.float32)]
    reduce_sum x2 -> x0, other arithmetic: 2.67 us -> none  [the longest x1 1.5 us: body(): local_sq = jnp.sum(xfloat * xfloat, axis=1)]
    reshape x0 -> x2, local copies, waits for them, and re-layouts: none -> 2.55 us  [the longest x1 1.28 us: fused_body(): norm_gain.reshape(1, depth)]
  transfers between devices with their start and end apart: 2 -> 0, of which waited for: 2 -> 0; matrix products, arithmetic and copies ran while one was open for 2% -> 0% of each run, Pallas kernels for 0% -> 0%
where the time goes in v2:
time: 77.2 us; the launch traced here: 77 us
  Pallas kernels  72.9 us (94%)
  local copies, waits for them, and re-layouts  4.12 us (5%)
    pallas_call x1, Pallas kernels, fused_body(): pl.pallas_call(functools.partial(kernel, n_ra, width, subs), out_shape=ja...  72.9 us
    unnamed x1, local copies, waits for them, and re-layouts  1.57 us

profile of v2, /device:TPU:0, one launch (start us, length us, event | category | flops | bytes accessed | tf_op | source)
XLA Modules:
  0.0 77.0 jit_solution(7138849768205021559)
XLA Ops:
  0.0 1.3 %reshape.6.refs_1_ = bf16[1,1024]{1,0:T(2,128)(2,1)} reshape(bf16[1024]{0:T(1024)(128)(2,1)} %param.7) | data formatting | bytes 4096 | tf_op jit(solution)/shard_map/reshape | solution.py:330
  1.3 1.3 %reshape.7.refs_5_ = bf16[1,1024]{1,0:T(2,128)(2,1)} reshape(bf16[1024]{0:T(1024)(128)(2,1)} %param.11) | data formatting | bytes 4096 | tf_op jit(solution)/shard_map/reshape | solution.py:330
  2.5 72.9 %shard_map.64 = bf16[64,1024]{1,0:T(8,128)(2,1)} custom-call(bf16[512,1024]{1,0:T(8,128)(2,1)} %refs_0_.1, bf16[1,1024]{1,0:T(2,128)(2,1)} %reshape.6.refs_1_, bf16[1024,1408]{1,0:T(8,128)(2,1)} %refs_2_.1, bf16[1024,1408]{1,0:T(8,128)(2,1)} %refs_3_.1, bf16[1408,1024]{1,0:T(8,128)(2,1)} %refs_4_.1, bf16[1,1024]{1,0:T(2,128)(2,1)} %reshape.7.refs_5_), custom_call_target="tpu_custom_call" | custom-call | tf_op jit(solution)/shard_map/pallas_call | solution.py:293
  75.4 1.6 %copy.8 = bf16[64,1024]{1,0:T(8,128)(2,1)} copy(bf16[64,1024]{1,0:T(8,128)(2,1)} %shard_map.64) | data formatting | bytes 262144

commit v3 on v2

--- a/solution.py
+++ b/solution.py
@@ -11,6 +11,7 @@
 LANES = 128
 TILE = 256
 PIECES = 3
+SLICES = 2
 SHARES = (1, 2, 2, 1, 1, 1)
 UNITS = sum(SHARES)
 VMEM_BYTES = 64 * 1024 * 1024 - 64 * 1024
@@ -62,7 +63,7 @@
     z_peers = [(lax.rem(z + d, nz) * 2 + y, cb) for d in range(1, nz)]
     mesh_id = pl.DeviceIdType.MESH
     pieces = column_pieces(2 * units)
-    halves = [(0, depth // 2), (depth // 2, depth // 2)]
+    slices = [(i * depth // SLICES, depth // SLICES) for i in range(SLICES)]
 
     early = [
         pltpu.make_async_copy(tok_hbm, tok, ld.at[0]),
@@ -151,7 +152,7 @@
             h2.wait_recv()
             hb = hid[k][...].reshape(n_ra * subs[k], units).astype(jnp.bfloat16)
             out = []
-            for h, (start, size) in enumerate(halves):
+            for h, (start, size) in enumerate(slices):
                 cols = pl.ds(start, size)
                 got = jnp.dot(hb, wd[:, cols], preferred_element_type=jnp.float32)
                 dn[k][:, :, :, cols] = got.reshape(2, nz, subs[k], size)
@@ -162,7 +163,7 @@
     def across(k, copies):
         with jax.named_scope(f"across{k}"):
             out = []
-            for h, (start, size) in enumerate(halves):
+            for h, (start, size) in enumerate(slices):
                 cols = pl.ds(start, size)
                 copies[h].wait_recv()
                 dn[k][y, :, :, cols] += yrec[k][:, :, cols]
@@ -192,11 +193,26 @@
             [xs[pl.ds((zz * 2 + yy) * own + base[k], subs[k]), :] for yy in range(2) for zz in range(nz)],
             axis=0).astype(jnp.bfloat16)
 
+    def squares():
+        with jax.named_scope("squares"):
+            lane = lax.broadcasted_iota(jnp.int32, (own, LANES), 1)
+            sqp[...] = jnp.zeros_like(sqp)
+            for d in range(n_ra):
+                xf = tok[pl.ds(d * own, own), :].astype(jnp.float32)
+                sq = jnp.broadcast_to(jnp.sum(xf * xf, axis=1, keepdims=True), (own, LANES))
+                for k in range(n):
+                    at = ((d % 2) * nz + d // 2) * subs[k]
+                    quarter = nz * subs[k] // 2
+                    q, off = at // quarter, at % quarter
+                    val = jnp.where(lane[:subs[k]] == k, sq[base[k]:base[k] + subs[k]], 0.0)
+                    sqp[q // 2, q % 2, pl.ds(off, subs[k]), :] += val
+            return send(sqp.at[oc], sqd, s_q.at[0], r_q.at[0], core_peer)
+
     with jax.named_scope("tokens"):
         for load in early:
             load.wait()
     with jax.named_scope("scale"):
-        gain = ng[...].astype(jnp.float32)
+        gain = ng[...].astype(jnp.float32).reshape(1, depth)
         for d in range(n_ra):
             at = pl.ds(d * own, own)
             xs[at, :] = tok[at, :].astype(jnp.float32) * gain
@@ -205,36 +221,28 @@
         pl.semaphore_wait(barrier, len(peers))
 
     a, b, h1, h2, hx, ys, zs, os = {}, {}, {}, {}, {}, {}, {}, {}
-    heads, b[0] = [], []
-    for p, (start, size) in enumerate(pieces):
-        with jax.named_scope("weights"):
-            for load in weights[p]:
-                load.wait()
-        project(0, p)
-        heads.append(to_core(0, pl.ds(start, size), p))
-        if p > 0:
-            b[0].append(combine(0, heads[p - 1], *pieces[p - 1], p - 1))
-    with jax.named_scope("squares"):
-        lane = lax.broadcasted_iota(jnp.int32, (own, LANES), 1)
-        sqp[...] = jnp.zeros_like(sqp)
-        for d in range(n_ra):
-            xf = tok[pl.ds(d * own, own), :].astype(jnp.float32)
-            sq = jnp.broadcast_to(jnp.sum(xf * xf, axis=1, keepdims=True), (own, LANES))
-            for k in range(n):
-                at = ((d % 2) * nz + d // 2) * subs[k]
-                quarter = nz * subs[k] // 2
-                q, off = at // quarter, at % quarter
-                val = jnp.where(lane[:subs[k]] == k, sq[base[k]:base[k] + subs[k]], 0.0)
-                sqp[q // 2, q % 2, pl.ds(off, subs[k]), :] += val
-        q1 = send(sqp.at[oc], sqd, s_q.at[0], r_q.at[0], core_peer)
-    last = len(pieces) - 1
-    b[0].append(combine(0, heads[last], *pieces[last], last))
-    fill(1)
-    a[1] = whole(1)
-    q1.wait_recv()
-    sqp[c] += sqd[...]
-    q2 = send(sqp.at[c, ox], sqx, s_q.at[1], r_q.at[1], x_peer)
-    b[1] = join(1, a[1])
+    b[0], b[1], waiting = [], [], []
+    for k in range(2):
+        for p, (start, size) in enumerate(pieces):
+            if k == 0:
+                with jax.named_scope("weights"):
+                    for load in weights[p]:
+                        load.wait()
+            project(k, p)
+            waiting.append((k, p, to_core(k, pl.ds(start, size), p)))
+            if k == 0 and p == 0:
+                q1 = squares()
+            if len(waiting) > 1:
+                kk, pp, copy = waiting.pop(0)
+                b[kk].append(combine(kk, copy, *pieces[pp], pp))
+            if k == 0 and p == 1:
+                with jax.named_scope("share"):
+                    q1.wait_recv()
+                    sqp[c] += sqd[...]
+                    q2 = send(sqp.at[c, ox], sqx, s_q.at[1], r_q.at[1], x_peer)
+                fill(1)
+    for kk, pp, copy in waiting:
+        b[kk].append(combine(kk, copy, *pieces[pp], pp))
     for k in range(2, n):
         fill(k)
     for load in late:
@@ -252,10 +260,15 @@
             b[t + 2] = join(t + 2, a[t + 2])
         if 0 <= t - 1 < n:
             h2[t - 1] = forward(t - 1, hx[t - 1])
+        if t == n and n > 2:
+            zs[n - 3] = across(n - 3, ys[n - 3])
+        if 0 <= t - 1 < n:
             ys[t - 1] = lower(t - 1, h1[t - 1], h2[t - 1])
-        if 0 <= t - 2 < n:
+        if t == n and n > 3:
+            os[n - 4] = finish(n - 4, zs[n - 4])
+        if 0 <= t - 2 < n and t != n - 1:
             zs[t - 2] = across(t - 2, ys[t - 2])
-        if 0 <= t - 3 < n:
+        if 0 <= t - 3 < n and t != n - 1:
             os[t - 3] = finish(t - 3, zs[t - 3])
     with jax.named_scope("norm"):
         for k in range(n):
@@ -263,7 +276,7 @@
                 copy.wait_recv()
         osum = osq[0] + osq[1] + osq[2] + osq[3]
         inv_out = lax.rsqrt(osum / width + EPS)[:, :1]
-        out_ref[...] = (mixed[...] * inv_out * og[...].astype(jnp.float32)).astype(out_ref.dtype)
+        out_ref[...] = (mixed[...] * inv_out * og[...].astype(jnp.float32).reshape(1, depth)).astype(out_ref.dtype)
     with jax.named_scope("drain"):
         for copy in sends:
             copy.wait_send()
@@ -298,8 +311,8 @@
         scratch_shapes=[
             pltpu.VMEM((count, depth), bf16),
             pltpu.VMEM((own, depth), bf16),
-            pltpu.VMEM((1, depth), bf16),
-            pltpu.VMEM((1, depth), bf16),
+            pltpu.VMEM((depth,), bf16),
+            pltpu.VMEM((depth,), bf16),
             pltpu.VMEM((depth, 2 * units), bf16),
             pltpu.VMEM((units, depth), bf16),
             pltpu.VMEM((count, depth), f32),
@@ -320,14 +333,14 @@
             dma((PIECES, 2)),
             *[dma((n, PIECES)) for _ in range(4)],
             *[dma((n, 3)) for _ in range(2)],
-            *[dma((n, 2)) for _ in range(2)],
-            *[dma((n, 2, nz - 1)) for _ in range(2)],
+            *[dma((n, SLICES)) for _ in range(2)],
+            *[dma((n, SLICES, nz - 1)) for _ in range(2)],
             *[dma((n, 3)) for _ in range(2)],
             *[dma((2,)) for _ in range(2)],
         ],
         compiler_params=pltpu.CompilerParams(
             collective_id=0, has_side_effects=True, vmem_limit_bytes=VMEM_BYTES),
-    )(tokens, norm_gain.reshape(1, depth), w_gate, w_up, w_down, out_gain.reshape(1, depth))
+    )(tokens, norm_gain, w_gate, w_up, w_down, out_gain)
 
 
 def solution(mesh):
@@ -340,7 +353,8 @@
         width = depth * n_cb
         tiled = (
             n_cb == 4 and n_ra % 4 == 0 and n_ra > 2
-            and count % (n_ra * UNITS * 8) == 0 and units % LANES == 0 and depth % TILE == 0)
+            and count % (n_ra * UNITS * 8) == 0 and units % LANES == 0 and depth % TILE == 0
+            and depth % (SLICES * LANES) == 0)
         if tiled:
             return fused_body(n_ra, width, *args)
         return plain_body(width, *args)

time: 77.2 us -> 74.2 us (0.961)
  local copies, waits for them, and re-layouts: 4.12 us -> 1.57 us
    reshape x2 -> x0, local copies, waits for them, and re-layouts: 2.55 us -> none  [the longest x1 1.28 us: fused_body(): norm_gain.reshape(1, depth)]
where the time goes in v3:
time: 74.2 us; the launch traced here: 74.1 us
  Pallas kernels  72.5 us (98%)
  local copies, waits for them, and re-layouts  1.57 us (2%)
    pallas_call x1, Pallas kernels, fused_body(): pl.pallas_call(functools.partial(kernel, n_ra, width, subs), out_shape=ja...  72.5 us
    unnamed x1, local copies, waits for them, and re-layouts  1.57 us

profile of v3, /device:TPU:0, one launch (start us, length us, event | category | flops | bytes accessed | tf_op | source)
XLA Modules:
  0.0 74.1 jit_solution(78842407787507723)
XLA Ops:
  0.0 72.5 %shard_map.64 = bf16[64,1024]{1,0:T(8,128)(2,1)} custom-call(bf16[512,1024]{1,0:T(8,128)(2,1)} %refs_0_.1, bf16[1024]{0:T(1024)(128)(2,1)} %refs_1_.1, bf16[1024,1408]{1,0:T(8,128)(2,1)} %refs_2_.1, bf16[1024,1408]{1,0:T(8,128)(2,1)} %refs_3_.1, bf16[1408,1024]{1,0:T(8,128)(2,1)} %refs_4_.1, bf16[1024]{0:T(1024)(128)(2,1)} %refs_5_.1), custom_call_target="tpu_custom_call" | custom-call | tf_op jit(solution)/shard_map/pallas_call | solution.py:306
  72.5 1.6 %copy.8 = bf16[64,1024]{1,0:T(8,128)(2,1)} copy(bf16[64,1024]{1,0:T(8,128)(2,1)} %shard_map.64) | data formatting | bytes 262144

commit v4 on v3

--- a/solution.py
+++ b/solution.py
@@ -146,18 +146,27 @@
             block = hid[k].at[c, ox]
             return send(block, block, s_h.at[k, 2], r_h.at[k, 2], core_peer)
 
+    def arrived(k, h1, h2):
+        h1.wait_recv()
+        h2.wait_recv()
+
+    def half(k, side):
+        return hid[k][side].reshape(n_ra * subs[k] // 2, units).astype(jnp.bfloat16)
+
     def lower(k, h1, h2):
         with jax.named_scope(f"lower{k}"):
-            h1.wait_recv()
-            h2.wait_recv()
-            hb = hid[k][...].reshape(n_ra * subs[k], units).astype(jnp.bfloat16)
+            pl.when(c != oy)(functools.partial(arrived, k, h1, h2))
+            rows = half(k, oy)
             out = []
             for h, (start, size) in enumerate(slices):
                 cols = pl.ds(start, size)
-                got = jnp.dot(hb, wd[:, cols], preferred_element_type=jnp.float32)
-                dn[k][:, :, :, cols] = got.reshape(2, nz, subs[k], size)
+                got = jnp.dot(rows, wd[:, cols], preferred_element_type=jnp.float32)
+                dn[k][oy, :, :, cols] = got.reshape(nz, subs[k], size)
                 out.append(send(dn[k].at[oy, :, :, cols], yrec[k].at[:, :, cols],
                                 s_y.at[k, h], r_y.at[k, h], y_peer))
+            pl.when(c == oy)(functools.partial(arrived, k, h1, h2))
+            got = jnp.dot(half(k, y), wd[...], preferred_element_type=jnp.float32)
+            dn[k][y] = got.reshape(nz, subs[k], depth)
             return out
 
     def across(k, copies):

time: 74.2 us -> 73.6 us (level)
  no operation moved by 1% of the time
where the time goes in v4:
time: 73.6 us; the launch traced here: 73.5 us
  Pallas kernels  71.9 us (98%)
  local copies, waits for them, and re-layouts  1.57 us (2%)
    pallas_call x1, Pallas kernels, fused_body(): pl.pallas_call(functools.partial(kernel, n_ra, width, subs), out_shape=ja...  71.9 us
    unnamed x1, local copies, waits for them, and re-layouts  1.57 us

profile of v4, /device:TPU:0, one launch (start us, length us, event | category | flops | bytes accessed | tf_op | source)
XLA Modules:
  0.0 73.5 jit_solution(2167521530069878375)
XLA Ops:
  0.0 71.9 %shard_map.64 = bf16[64,1024]{1,0:T(8,128)(2,1)} custom-call(bf16[512,1024]{1,0:T(8,128)(2,1)} %refs_0_.1, bf16[1024]{0:T(1024)(128)(2,1)} %refs_1_.1, bf16[1024,1408]{1,0:T(8,128)(2,1)} %refs_2_.1, bf16[1024,1408]{1,0:T(8,128)(2,1)} %refs_3_.1, bf16[1408,1024]{1,0:T(8,128)(2,1)} %refs_4_.1, bf16[1024]{0:T(1024)(128)(2,1)} %refs_5_.1), custom_call_target="tpu_custom_call" | custom-call | tf_op jit(solution)/shard_map/pallas_call | solution.py:315
  71.9 1.6 %copy.8 = bf16[64,1024]{1,0:T(8,128)(2,1)} copy(bf16[64,1024]{1,0:T(8,128)(2,1)} %shard_map.64) | data formatting | bytes 262144
